TPU v7x, 32 devices: a whole 2x2x4 slice. The times are simulated.
32 devices in a mesh: kv: 8 (over z, y), tp: 4 (over x, core).
Axes of the slice: x: 2, y: 2, z: 4, core: 2. Of those that a mesh axis runs over, the one named last changes fastest.
Arguments:
- layer_input: bfloat16 [4, 4096, 2048], P(None, 'kv', 'tp'), may hold values from -0.119628906 to 0.119628906
- queries: bfloat16 [4, 4096, 2048], P(None, 'kv', 'tp'), may hold values from -3.5 to 3.5
- keys: bfloat16 [4, 4096, 2048], P(None, 'kv', 'tp'), may hold values from -3.5 to 3.5
- values: bfloat16 [4, 4096, 2048], P(None, 'kv', 'tp'), may hold values from -5 to 5
- outputs: bfloat16 [4, 4096, 2048], P(None, 'kv', 'tp'), may hold values from -1.5 to 1.5
- d_out: bfloat16 [4, 4096, 2048], P(None, 'kv', 'tp'), may hold values from -30 to 30
- log_sums: float32 [4, 4096, 16], P(None, 'kv', 'tp'), may hold values from 6 to 8
- chosen: int32 [4, 64, 12], P(None, 'kv'), may hold values from -1 to 63, as said below
Outputs:
- d_queries: bfloat16 [4, 4096, 2048], P(None, 'kv', 'tp')
- d_keys: bfloat16 [4, 4096, 2048], P(None, 'kv', 'tp')
- d_values: bfloat16 [4, 4096, 2048], P(None, 'kv', 'tp')
- d_weight: float32 [2048, 2048], P('kv', 'tp')
Inputs may be any that keep to these rules, and one draw needn't show every extreme that they name: Row chosen[s, b] names key blocks of sequence s for query block b: its first entry is b itself, the others are distinct blocks with smaller indices, either on the same device as b or on earlier devices; -1 marks unused slots, which come last. Over all sequences, the blocks of one device that query blocks of other devices name are at most 2, and in every draw some devices' are exactly 2.
All inputs are finite; a program needn't handle non-finite values.
Results may differ from a plain program's by a relative error of at most 0.0055.
Values may be sent and summed in bfloat16 or wider, within the bound.
A program may use at most 256 MiB of HBM per device.

v0:
```python
import functools

import jax
import jax.numpy as jnp
from jax import lax
from jax.experimental import pallas as pl
from jax.experimental.pallas import tpu as pltpu
from jax.sharding import PartitionSpec as P

BLK = 64
SEL = 12
CAP = 2
LOG2E = 1.4426950408889634
HIDDEN = 1e30
GROUP = 4

NT = (((1,), (1,)), ((), ()))
NN = (((1,), (0,)), ((), ()))
TN = (((0,), (0,)), ((), ()))


def dot(a, b, dims):
    return lax.dot_general(a, b, dims, preferred_element_type=jnp.float32)


def pair_terms(k, v, q, g, shift_rows, delta_row, scale, diagonal):
    count = q.shape[0]
    shift = jnp.concatenate([jnp.broadcast_to(r, (BLK, count)) for r in shift_rows], axis=0)
    prob = jnp.exp2(dot(k, q, NT) * (scale * LOG2E) - shift)
    if diagonal:
        rows = lax.broadcasted_iota(jnp.int32, prob.shape, 0)
        cols = lax.broadcasted_iota(jnp.int32, prob.shape, 1)
        prob = jnp.where(rows <= cols, prob, 0.0)
    dscore = prob * (dot(v, g, NT) - delta_row)
    prob = prob.astype(jnp.bfloat16)
    dscore = dscore.astype(jnp.bfloat16)
    return dot(dscore, k, TN), dot(dscore, q, NN) * scale, dot(prob, g, NN)


def peer(index, axis="kv"):
    return dict(device_id={axis: index}, device_id_type=pl.DeviceIdType.MESH)


def meet(others, across=()):
    barrier = pltpu.get_barrier_semaphore()
    for other in others:
        pl.semaphore_signal(barrier, inc=1, **peer(other))
    for other in across:
        pl.semaphore_signal(barrier, inc=1, **peer(other, "tp"))
    pl.semaphore_wait(barrier, len(others) + len(across))


def places_of(devices, axis="kv"):
    me = lax.axis_index(axis)
    inner = 2 if devices % 2 == 0 else 1
    outer = devices // inner
    a, b = me // inner, me % inner
    onward = [lax.rem(a + 1 + i, outer) for i in range(outer)]
    source = [lax.rem(a + outer - 1 - i, outer) for i in range(outer)]
    return me, inner, outer, a, b, onward, source


def spread_kernel(devices, mine_ref, all_ref, send_sem, recv_sem):
    me = lax.axis_index("kv")
    others = [lax.rem(me + i, devices) for i in range(1, devices)]
    meet(others)
    copies = []
    for i, other in enumerate(others):
        copy = pltpu.make_async_remote_copy(
            mine_ref, all_ref.at[me], send_sem.at[i], recv_sem.at[i], **peer(other)
        )
        copy.start()
        copies.append(copy)
    all_ref[pl.ds(me, 1)] = mine_ref[...][None]
    for copy in copies:
        copy.wait()


def spread(chosen, devices):
    return pl.pallas_call(
        functools.partial(spread_kernel, devices),
        out_shape=jax.ShapeDtypeStruct((devices,) + chosen.shape, chosen.dtype),
        in_specs=[pl.BlockSpec(memory_space=pltpu.VMEM)],
        out_specs=pl.BlockSpec(memory_space=pltpu.VMEM),
        scratch_shapes=[pltpu.SemaphoreType.DMA((devices - 1,)), pltpu.SemaphoreType.DMA((devices - 1,))],
        compiler_params=pltpu.CompilerParams(collective_id=0, has_side_effects=True),
        name="spread_choice",
    )(chosen)


def total_kernel(devices, width, *refs):
    if width:
        terms_ref, x_ref, _, out_ref, whole_ref = refs[:5]
        scratch = refs[5:12]
        half = x_ref.shape[0] // 2
        keep, (x_own, x_far, x_onto, across) = input_copies(
            width, half, x_ref.shape[0] - half, x_ref, whole_ref, *refs[12:]
        )
    else:
        terms_ref, out_ref = refs[:2]
        scratch = refs[2:]
        across = ()
    near_in, far_out, far_in, near_send, near_recv, far_send, far_recv = scratch
    me, inner, outer, a, b, onward, _ = places_of(devices)
    partner = a * inner + (1 - b)
    meet([partner] + [place * inner + b for place in onward[:-1]], across)
    near, far = [], []
    for i, place in enumerate(onward):
        copy = pltpu.make_async_remote_copy(
            terms_ref.at[place * inner + (1 - b)], near_in.at[i],
            near_send.at[i], near_recv.at[i], **peer(partner),
        )
        copy.start()
        near.append(copy)
    if width:
        for copy in x_far + [x_own, keep]:
            copy.start()
    for i, place in enumerate(onward):
        near[i].wait_recv()
        both = terms_ref[place * inner + b].astype(jnp.float32) + near_in[i].astype(jnp.float32)
        if i == outer - 1:
            out_ref[...] = both
            break
        far_out[i] = both.astype(jnp.bfloat16)
        copy = pltpu.make_async_remote_copy(
            far_out.at[i], far_in.at[i], far_send.at[i], far_recv.at[i],
            **peer(place * inner + b),
        )
        copy.start()
        far.append(copy)
    if width:
        for i in range(len(x_far)):
            x_far[i].wait_recv()
            x_onto[i].start()
    for i, copy in enumerate(far):
        copy.wait_recv()
        out_ref[...] += far_in[i].astype(jnp.float32)
    for copy in near + far:
        copy.wait_send()
    if width:
        keep.wait()
        x_own.wait()
        for copy in x_far:
            copy.wait_send()
        for copy in x_onto:
            copy.wait()


def total(terms, ident, label, layer_input=None, whole=None):
    devices, rows, columns = terms.shape
    outer = devices // 2
    dma = pltpu.SemaphoreType.DMA
    vmem, anywhere = pl.BlockSpec(memory_space=pltpu.VMEM), pl.BlockSpec(memory_space=pl.ANY)
    out_shape = [jax.ShapeDtypeStruct((rows, columns), jnp.float32)]
    scratch = [
        pltpu.VMEM((outer, rows, columns), jnp.bfloat16),
        pltpu.VMEM((outer - 1, rows, columns), jnp.bfloat16),
        pltpu.VMEM((outer - 1, rows, columns), jnp.bfloat16),
        dma((outer,)), dma((outer,)), dma((outer - 1,)), dma((outer - 1,)),
    ]
    width, more, aliases = 0, [], {}
    if whole is not None:
        width = whole.shape[0]
        more, aliases = [layer_input, whole], {2: 1}
        out_shape.append(jax.ShapeDtypeStruct(whole.shape, whole.dtype))
        scratch += [dma] + gather_sems(width)
    return pl.pallas_call(
        functools.partial(total_kernel, devices, width),
        out_shape=out_shape,
        in_specs=[vmem] + [anywhere] * len(more),
        out_specs=[vmem] + [anywhere] * (len(out_shape) - 1),
        scratch_shapes=scratch,
        input_output_aliases=aliases,
        compiler_params=pltpu.CompilerParams(collective_id=ident, has_side_effects=True),
        name=label,
    )(terms, *more)


def gather_copies(devices, axis, mine, pool, own_send, own_recv, far_send, far_recv, pass_send, pass_recv):
    me, inner, outer, a, b, onward, source = places_of(devices, axis)
    partner = a * inner + (1 - b)
    own = pltpu.make_async_remote_copy(mine, pool(me), own_send, own_recv, **peer(partner, axis))
    far = [
        pltpu.make_async_remote_copy(
            mine, pool(me), far_send.at[i], far_recv.at[i], **peer(onward[i] * inner + b, axis)
        )
        for i in range(outer - 1)
    ]
    onto = [
        pltpu.make_async_remote_copy(
            pool(source[i] * inner + b), pool(source[i] * inner + b),
            pass_send.at[i], pass_recv.at[i], **peer(partner, axis),
        )
        for i in range(outer - 1)
    ]
    others = [partner] + [onward[i] * inner + b for i in range(outer - 1)]
    return own, far, onto, others


def gather_sems(devices):
    dma, hops = pltpu.SemaphoreType.DMA, devices // 2 - 1
    return [dma, dma, dma((hops,)), dma((hops,)), dma((hops,)), dma((hops,))]


def input_copies(width, start, count, x_ref, whole_ref, keep_sem, *sems):
    part = pl.ds(start, count)
    keep = pltpu.make_async_copy(x_ref.at[part], whole_ref.at[lax.axis_index("tp"), part], keep_sem)
    return keep, gather_copies(
        width, "tp", x_ref.at[part], lambda place: whole_ref.at[place, part], *sems
    )


def local_kernel(devices, width, steps, scale, mine_ref, x_ref, q_ref, k_ref, v_ref, o_ref, g_ref, log_ref, hide_ref,
                 dq_ref, dk_ref, dv_ref, delta_ref, pool_ref, whole_ref, *sems):
    positions = q_ref.shape[1]
    step = pl.program_id(0) * pl.num_programs(1) + pl.program_id(1)
    own, far, onto, others = gather_copies(
        devices, "kv", mine_ref, lambda place: pool_ref.at[place], *sems[:6]
    )
    keep, (x_own, x_far, x_onto, across) = input_copies(
        width, 0, x_ref.shape[0] // 2, x_ref, whole_ref, *sems[6:]
    )

    @pl.when(step == 0)
    def _():
        meet(others, across)
        for copy in far:
            copy.start()
        own.start()
        for copy in x_far + [x_own, keep]:
            copy.start()

    for i in range(len(far)):
        @pl.when(step == (i + 1) * steps // (len(far) + 1))
        def _(i=i):
            far[i].wait_recv()
            onto[i].start()

    product = g_ref[0].astype(jnp.float32) * o_ref[0].astype(jnp.float32)
    delta = jnp.sum(product.T, axis=0, keepdims=True)
    delta_ref[0, 0] = delta
    log_row = log_ref[0, 0]
    chunk = GROUP * BLK
    for start in range(0, positions, chunk):
        keys = slice(start, start + chunk)
        rest = slice(start, positions)
        shifts = [
            log_row[:, rest] + hide_ref[0, start // BLK + i : start // BLK + i + 1, rest]
            for i in range(GROUP)
        ]
        dq, dk, dv = pair_terms(
            k_ref[0, keys], v_ref[0, keys], q_ref[0, rest], g_ref[0, rest],
            shifts, delta[:, rest], scale, True,
        )
        if start == 0:
            dq_ref[0] = dq
        else:
            dq_ref[0, rest] += dq
        dk_ref[0, keys] = dk.astype(jnp.bfloat16)
        dv_ref[0, keys] = dv.astype(jnp.bfloat16)

    @pl.when(step == steps - 1)
    def _():
        own.wait()
        for copy in far:
            copy.wait_send()
        for copy in x_far:
            copy.wait_recv()
        for copy in x_onto:
            copy.start()
        for copy in onto:
            copy.wait()
        keep.wait()
        x_own.wait()
        for copy in x_far:
            copy.wait_send()
        for copy in x_onto:
            copy.wait()


def remote_kernel(scale, order_ref, read_ref, chunks_ref, pool_ref, hide_ref, q_ref, g_ref, log_ref,
                  delta_ref, base_ref, dq_ref, out_ref, total):
    s = pl.program_id(1)

    @pl.when(s == 0)
    def _():
        out_ref[...] = jnp.zeros_like(out_ref)

    total[...] = base_ref[0]

    @pl.loop(0, chunks_ref[s])
    def _(c):
        slots = [order_ref[s, c * GROUP + i] for i in range(GROUP)]
        places = [(lax.div(r, CAP), lax.rem(r, CAP)) for r in slots]
        reads = [read_ref[s, c * GROUP + i] for i in range(GROUP)]
        reads = [(lax.div(r, CAP), lax.rem(r, CAP)) for r in reads]
        k = jnp.concatenate([pool_ref[o, 0, n] for o, n in reads], axis=0)
        v = jnp.concatenate([pool_ref[o, 1, n] for o, n in reads], axis=0)
        shifts = [log_ref[0, 0] + hide_ref[r] for r in slots]
        dq, dk, dv = pair_terms(
            k, v, q_ref[0], g_ref[0], shifts, delta_ref[0, 0], scale, False
        )
        total[...] += dq
        dk = dk.astype(jnp.bfloat16)
        dv = dv.astype(jnp.bfloat16)
        for i, (o, n) in enumerate(places):
            out_ref[o, 0, n] = dk[i * BLK : (i + 1) * BLK]
            out_ref[o, 1, n] = dv[i * BLK : (i + 1) * BLK]

    dq_ref[0] = (total[...] * scale).astype(jnp.bfloat16)


def body(layer_input, queries, keys, values, outputs, d_out, log_sums, chosen):
    sequences, positions, channels = queries.shape
    head_count = log_sums.shape[2]
    head_size = channels // head_count
    local_blocks = positions // BLK
    devices = lax.axis_size("kv")
    me = lax.axis_index("kv")
    own_blocks = sequences * local_blocks
    slots = devices * CAP
    scale = head_size ** (-0.5)
    bf16, f32, i32 = jnp.bfloat16, jnp.float32, jnp.int32

    every = spread(chosen, devices).transpose(1, 0, 2, 3).reshape(sequences, -1, chosen.shape[2])
    width = lax.axis_size("tp")

    total_blocks = devices * local_blocks
    ids = jnp.arange(total_blocks, dtype=i32)
    asker = ids // local_blocks
    named = (every[..., None] == ids) & (
        asker[None, :, None, None] != asker[None, None, None, :]
    )
    needed = jnp.any(named, axis=(1, 2))
    needed = needed.reshape(sequences, devices, local_blocks).transpose(1, 0, 2)
    needed = needed.reshape(devices, own_blocks)
    place = jnp.where(needed, jnp.arange(own_blocks, dtype=i32), own_blocks)
    table = []
    for _ in range(CAP):
        first = jnp.min(place, axis=1)
        table.append(first)
        place = jnp.where(place == first[:, None], own_blocks, place)
    table = jnp.stack(table, axis=1)
    served = lax.dynamic_slice_in_dim(table, me, 1, 0).reshape(CAP)
    served = jnp.where(served < own_blocks, served, 0)

    key_rows = keys.reshape(own_blocks, BLK, channels)
    value_rows = values.reshape(own_blocks, BLK, channels)
    sent = jnp.stack([
        jnp.stack([lax.dynamic_index_in_dim(rows, served[n], 0, False) for n in range(CAP)])
        for rows in (key_rows, value_rows)
    ])

    slot_place = table.reshape(slots)
    slot_owner = jnp.arange(slots, dtype=i32) // CAP
    slot_ok = (slot_place < own_blocks) & (slot_owner != me)
    slot_seq = jnp.where(slot_ok, slot_place // local_blocks, -1)
    slot_block = slot_owner * local_blocks + slot_place % local_blocks
    seqs = jnp.arange(sequences, dtype=i32)
    sees = jnp.any(chosen[..., None] == slot_block, axis=2) & (
        slot_seq[None, None, :] == seqs[:, None, None]
    )
    seen = jnp.any(sees, axis=0)
    remote_hide = jnp.where(seen.T, 0.0, HIDDEN).astype(f32)
    remote_hide = jnp.repeat(remote_hide, BLK, axis=1).reshape(slots, 1, positions)
    match = jnp.any(sees, axis=1)
    line = jnp.arange(slots, dtype=i32)
    rank = jnp.sum((match[:, None, :] & (line[None, None, :] < line[None, :, None])).astype(i32), axis=2)
    count = jnp.sum(match.astype(i32), axis=1)
    chunks = (count + GROUP - 1) // GROUP
    padded = -(-slots // GROUP) * GROUP
    steps = jnp.arange(padded, dtype=i32)
    hits = match[:, None, :] & (rank[:, None, :] == steps[None, :, None])
    order = jnp.sum(jnp.where(hits, line[None, None, :], 0), axis=2)
    filled = steps[None, :] < count[:, None]
    read = jnp.where(filled, order, (me ^ 1) * CAP)
    order = jnp.where(filled, order, me * CAP)

    mine = me * local_blocks + jnp.arange(local_blocks, dtype=i32)
    near = jnp.any(chosen[..., None] == mine, axis=2)
    local_hide = jnp.where(near.transpose(0, 2, 1), 0.0, HIDDEN).astype(f32)
    local_hide = jnp.repeat(local_hide, BLK, axis=2)
    log_rows = (log_sums * LOG2E).transpose(0, 2, 1)[:, :, None, :]

    tile = pl.BlockSpec((1, positions, head_size), lambda s, h: (s, 0, h))
    row = pl.BlockSpec((1, 1, 1, positions), lambda s, h: (s, h, 0, 0))
    shape = (sequences, positions, channels)
    flops = 10 * sequences * head_count * positions * positions * head_size
    anywhere = pl.BlockSpec(memory_space=pl.ANY)
    dq_local, dk_local, dv_local, delta_rows, pool, whole_input = pl.pallas_call(
        functools.partial(local_kernel, devices, width, sequences * head_count, scale),
        grid=(sequences, head_count),
        in_specs=[anywhere] * 2 + [tile] * 5 + [row, pl.BlockSpec((1, local_blocks, positions), lambda s, h: (s, 0, 0))],
        out_specs=[tile, tile, tile, row, anywhere, anywhere],
        out_shape=[
            jax.ShapeDtypeStruct(shape, f32),
            jax.ShapeDtypeStruct(shape, bf16),
            jax.ShapeDtypeStruct(shape, bf16),
            jax.ShapeDtypeStruct((sequences, head_count, 1, positions), f32),
            jax.ShapeDtypeStruct((devices, 2, CAP, BLK, channels), bf16),
            jax.ShapeDtypeStruct((width,) + layer_input.shape, bf16),
        ],
        scratch_shapes=gather_sems(devices) + [pltpu.SemaphoreType.DMA] + gather_sems(width),
        compiler_params=pltpu.CompilerParams(collective_id=1, has_side_effects=True),
        cost_estimate=pl.CostEstimate(flops=4 * flops, bytes_accessed=queries.size * 18, transcendentals=0),
        name="near_terms",
    )(sent, layer_input, queries, keys, values, outputs, d_out, log_rows, local_hide)

    tile_t = pl.BlockSpec((1, positions, head_size), lambda h, s, *_: (s, 0, h))
    row_t = pl.BlockSpec((1, 1, 1, positions), lambda h, s, *_: (s, h, 0, 0))
    pool_t = pl.BlockSpec((devices, 2, CAP, BLK, head_size), lambda h, s, *_: (0, 0, 0, 0, h))
    d_queries, terms = pl.pallas_call(
        functools.partial(remote_kernel, scale),
        grid_spec=pltpu.PrefetchScalarGridSpec(
            num_scalar_prefetch=3,
            grid=(head_count, sequences),
            in_specs=[
                pool_t,
                pl.BlockSpec((slots, 1, positions), lambda h, s, *_: (0, 0, 0)),
                tile_t, tile_t, row_t, row_t, tile_t,
            ],
            out_specs=[tile_t, pool_t],
            scratch_shapes=[pltpu.VMEM((positions, head_size), f32)],
        ),
        out_shape=[
            jax.ShapeDtypeStruct(shape, bf16),
            jax.ShapeDtypeStruct((devices, 2, CAP, BLK, channels), bf16),
        ],
        cost_estimate=pl.CostEstimate(flops=2 * flops, bytes_accessed=queries.size * 10, transcendentals=0),
        name="far_terms",
    )(order, read, chunks, pool, remote_hide, queries, d_out, log_rows, delta_rows, dq_local)

    returned, whole_input = total(
        terms.reshape(devices, 2 * CAP * BLK, channels), 2, "return_terms", layer_input, whole_input
    )
    returned = returned.reshape(2, CAP, BLK, channels)

    def settle(rows, back):
        rows = rows.reshape(own_blocks, BLK, channels).astype(f32)
        block = jnp.arange(own_blocks, dtype=i32)[:, None, None]
        for n in range(CAP):
            rows = rows + jnp.where(block == served[n], back[n][None], 0.0)
        return rows.astype(bf16).reshape(shape)

    d_keys = settle(dk_local, returned[0])
    d_values = settle(dv_local, returned[1])
    input_rows = whole_input.reshape(-1, sequences * positions, layer_input.shape[2])
    partial = jnp.einsum(
        "pti,tj->pij", input_rows, d_values.reshape(sequences * positions, channels),
        preferred_element_type=f32,
    ).astype(bf16).reshape(devices, -1, channels)
    d_weight, = total(partial, 3, "weight_terms")
    return (d_queries, d_keys, d_values, d_weight)


def solution(mesh):
    split = P(None, "kv", "tp")
    return jax.shard_map(
        body,
        mesh=mesh,
        in_specs=(split,) * 7 + (P(None, "kv", None),),
        out_specs=(split, split, split, P("kv", "tp")),
        check_vma=False,
    )
```

profile of v0, /device:TPU:10, one launch (start us, length us, event | category | flops | bytes accessed | tf_op | source)
XLA Modules:
  0.0 180.1 jit_solution(1006746769882178746)
XLA Ops:
  0.7 1.4 compare_reduce_fusion.1
  2.3 0.8 multiply_bitcast_fusion
  3.0 0.6 broadcast_in_dim.187.log_ref
  3.7 0.8 copy.19
  4.6 0.7 reshape.319.hide_ref
  5.3 8.6 %spread_choice.1 = s32[8,4,8,12]{3,2,1,0:T(8,128)} custom-call(s32[4,8,12]{2,1,0:T(8,128)} %mine_ref.1), custom_call_target="tpu_custom_call" | custom-call | tf_op jit(solution)/shard_map/spread_choice/pallas_call | solution.py:80
  13.9 1.2 copy.28
  15.2 0.6 fusion.8
  16.5 0.6 fusion.18
  20.9 0.7 fusion.14
  21.6 0.7 fusion.13
  23.0 0.6 and_select_fusion.chunks_ref
  23.6 0.6 fusion.11
  24.8 0.7 reshape_reshape.4.hide_ref
  25.5 1.0 constant_dynamic-slice_fusion.1
  26.5 0.7 pad_maximum_fusion.mine_ref
  27.2 37.7 %near_terms.1 = (f32[4,512,512]{2,1,0:T(8,128)}, bf16[4,512,512]{2,1,0:T(8,128)(2,1)}, bf16[4,512,512]{2,1,0:T(8,128)(2,1)}, f32[4,4,1,512]{3,2,1,0:T(1,128)}, b...) custom-call(bf16[2,2,64,512]{3,2,1,0:T(8,128)(2,1)} %pad_maximum_fusion.mine_ref, ...), custom_call_target="tpu_custom_call" | custom-call | flops 21474836480 | bytes 18874368 | tf_op jit(solution)/shard_map/near_terms/pallas_call | solution.py:390
  64.9 18.4 %far_terms.1 = (bf16[4,512,512]{2,1,0:T(8,128)(2,1)}, bf16[8,2,2,64,512]{4,3,2,1,0:T(8,128)(2,1)}) custom-call(s32[4,16]{1,0:T(4,128)} %get-tuple-element.37.order_ref, s32[4,16]{1,0:T(4,128)} %get-tuple-element.36.read_ref, s32[4]{0:T(128)} %and_select_fusion.chunks_ref, bf16[8,2,2,64,512]{4,3,2,1,0:T(8,128)(2,1)} %get-tuple-element.14.pool_ref, ...), custom_call_target="tpu_custom_call" | custom-call | flops 10737418240 | bytes 10485760 | tf_op jit(solution)/shard_map/far_terms/pallas_call | solution.py:412
  83.3 42.1 %return_terms.1 = (f32[256,512]{1,0:T(8,128)}, bf16[4,4,512,512]{3,2,1,0:T(8,128)(2,1)}) custom-call(bf16[8,256,512]{2,1,0:T(8,128)(2,1)} %bitcast.71, bf16[4,512,512]{2,1,0:T(8,128)(2,1)} %refs_1_.1, bf16[4,4,512,512]{3,2,1,0:T(8,128)(2,1)} %get-tuple-element.20.refs_2_), custom_call_target="tpu_custom_call", output_to_operand_aliasing={{1}: (2, {})} | custom-call | tf_op jit(solution)/shard_map/return_terms/pallas_call | solution.py:167
  125.5 1.1 fusion.17
  129.3 4.7 %fusion.1 = (bf16[4,512,512]{2,1,0:T(8,128)(2,1)}, bf16[4,512,512]{2,1,0:T(8,128)(2,1)}) fusion(bf16[4,512,512]{2,1,0:T(8,128)(2,1)} %get-tuple-element.22, pred[4,512]{1,0:T(4,128)(4,1)S(1)} %broadcast_in_dim.201, pred[4,512]{1,0:T(4,128)(4,1)S(1)} %broadcast_in_dim.195, bf16[4,512,512]{2,1,0:T(8,128)(2,1)S(1)} %copy-done, f32[4,512,512]{2,1,0:T(8,128)S(1)} %bitcast.65, ...), kind=kLoop, calls=%fused_computation.3 | loop fusion | flops 12582912 | bytes 25169920 | tf_op jit(solution)/shard_map/convert_element_type | solution.py:443
  134.0 7.4 %bitcast_convert_fusion = bf16[4,512,512]{2,1,0:T(8,128)(2,1)} fusion(bf16[4,4,512,512]{3,2,1,0:T(8,128)(2,1)S(1)} %bitcast.69, bf16[4,512,512]{2,1,0:T(8,128)(2,1)} %get-tuple-element.50), kind=kOutput, calls=%fused_computation | convolution fusion | flops 4296015872 | bytes 12582912 | tf_op jit(solution)/shard_map/pti,tj->pij/dot_general | solution.py:448
  141.3 36.9 %weight_terms.1 = f32[256,512]{1,0:T(8,128)} custom-call(bf16[8,256,512]{2,1,0:T(8,128)(2,1)} %bitcast.70), custom_call_target="tpu_custom_call" | custom-call | tf_op jit(solution)/shard_map/weight_terms/pallas_call | solution.py:167
  178.3 1.9 %copy.32 = f32[256,512]{1,0:T(8,128)} copy(f32[256,512]{1,0:T(8,128)} %weight_terms.1) | data formatting | bytes 1048576
  (44 shorter events, 4.9 us)
Async XLA Ops:
  127.7 1.6 copy-start
  128.2 5.7 %slice-start = ((s8[8388608]{0:T(1024)(128)(4,1)}), s8[4194304]{0:T(1024)(128)(4,1)S(1)}, s32[]{:S(2)}) async-start(s8[8388608]{0:T(1024)(128)(4,1)} %bitcast.68), calls=%async_computation | async-start | bytes 8388608
  129.3 4.7 %slice-start.1 = ((s8[8388608]{0:T(1024)(128)(4,1)}), s8[4194304]{0:T(1024)(128)(4,1)S(1)}, s32[]{:S(2)}) async-start(s8[8388608]{0:T(1024)(128)(4,1)} %bitcast.68), calls=%async_computation.1 | async-start | bytes 8388608
where the time goes:
time: 183 us; the launch traced here: 180 us
  Pallas kernels  144 us (79%)
  local copies, waits for them, and re-layouts  12.4 us (7%)
  other arithmetic  11.8 us (6%)
  matrix products  7.35 us (4%)
  between operations  4.75 us (3%)
    pallas_call x2, Pallas kernels, total(): pl.pallas_call(functools.partial(total_kernel, devices, width), out_shape...  79.1 us
    pallas_call x1, Pallas kernels, body(): pl.pallas_call(functools.partial(local_kernel, devices, width, sequences...  37.7 us
    pallas_call x1, Pallas kernels, body(): pl.pallas_call(functools.partial(remote_kernel, scale), grid_spec=pltpu.P...  18.4 us
    pallas_call x1, Pallas kernels, spread(): pl.pallas_call(functools.partial(spread_kernel, devices), out_shape=jax.S...  8.63 us
    dot_general x1, matrix products, body(): jnp.einsum('pti,tj->pij', input_rows, d_values.reshape(sequences * positi...  7.35 us
    convert_element_type x1, other arithmetic, settle(): return rows.astype(bf16).reshape(shape)  4.68 us

commit v1 on v0

v1 whole, which is shorter than its diff:
```python
import functools

import jax
import jax.numpy as jnp
from jax import lax
from jax.experimental import pallas as pl
from jax.experimental.pallas import tpu as pltpu
from jax.sharding import PartitionSpec as P

BLK = 64
CAP = 2
LOG2E = 1.4426950408889634
HIDDEN = 1e30
GROUP = 4
BATCH = 8
NONE = 1 << 20

NT = (((1,), (1,)), ((), ()))
NN = (((1,), (0,)), ((), ()))
TN = (((0,), (0,)), ((), ()))
bf16, f32, i32 = jnp.bfloat16, jnp.float32, jnp.int32


def dot(a, b, dims):
    return lax.dot_general(a, b, dims, preferred_element_type=f32)


def peer(index, axis="kv"):
    return dict(device_id={axis: index}, device_id_type=pl.DeviceIdType.MESH)


def remote(source, target, send, recv, index, axis="kv"):
    return pltpu.make_async_remote_copy(source, target, send, recv, **peer(index, axis))


def probabilities(k, v, q, g, shift, delta, scale, diagonal):
    prob = jnp.exp2(dot(k, q, NT) * (scale * LOG2E) - shift)
    if diagonal:
        rows = lax.broadcasted_iota(i32, prob.shape, 0)
        cols = lax.broadcasted_iota(i32, prob.shape, 1)
        prob = jnp.where(rows <= cols, prob, 0.0)
    dscore = prob * (dot(v, g, NT) - delta)
    return prob.astype(bf16), dscore.astype(bf16)


def kernel(
    devices, width, heads, scale,
    x_hbm, q_hbm, k_hbm, v_hbm, o_hbm, g_hbm, log_ref, chosen_ref,
    dq_hbm, dk_hbm, dv_hbm, dw_hbm,
    every, q, k, v, o, g, x, dq, dk, dv, delta, pool, dscore, terms, back_in, back_far, part, part_in,
    part_far, dw, table,
    load_sem, keep_sem, out_sem, every_send, every_recv, x_send, x_recv,
    own_send, own_recv, chain_send, chain_recv, pass_send, pass_recv,
    back_send, back_recv, home_send, home_recv, part_send, part_recv, sum_send, sum_recv,
):
    sequences, positions, channels = q.shape
    size = channels // heads
    blocks = positions // BLK
    outer = devices // 2
    me, lane = lax.axis_index("kv"), lax.axis_index("tp")
    a, b = me // 2, me % 2
    partner = a * 2 + (1 - b)
    core = lane // 2 * 2 + (1 - lane % 2)
    head = [slice(h * size, (h + 1) * size) for h in range(heads)]

    def load(j, s):
        source, target = ((k_hbm, k), (v_hbm, v), (q_hbm, q), (g_hbm, g), (o_hbm, o))[j]
        return pltpu.make_async_copy(source.at[s], target.at[s], load_sem.at[j, s])

    for j in range(5):
        for s in range(sequences):
            load(j, s).start()
    keep = pltpu.make_async_copy(x_hbm, x.at[lane], keep_sem)
    keep.start()

    barrier = pltpu.get_barrier_semaphore()
    for i in range(1, devices):
        pl.semaphore_signal(barrier, inc=1, **peer(lax.rem(me + i, devices)))
    for i in range(1, width):
        pl.semaphore_signal(barrier, inc=1, **peer(lax.rem(lane + i, width), "tp"))
    pl.semaphore_wait(barrier, devices + width - 2)

    asks = [
        remote(chosen_ref, every.at[me], every_send.at[i - 1], every_recv.at[i - 1], lax.rem(me + i, devices))
        for i in range(1, devices)
    ]
    for ask in asks:
        ask.start()
    x_far = [
        remote(x_hbm, x.at[lane], x_send.at[i - 1], x_recv.at[i - 1], lax.rem(lane + 2 * i, width), "tp")
        for i in range(1, width // 2)
    ]
    x_own = remote(x_hbm, x.at[lane], x_send.at[width - 2], x_recv.at[width - 2], core, "tp")
    x_onto = []
    for i in range(1, width // 2):
        origin = lax.rem(lane + width - 2 * i, width)
        at = width // 2 - 2 + i
        x_onto.append(remote(x.at[origin], x.at[origin], x_send.at[at], x_recv.at[at], core, "tp"))
    for copy in x_far + [x_own]:
        copy.start()
    every[pl.ds(me, 1)] = chosen_ref[...][None]

    seq_of = lax.broadcasted_iota(i32, (sequences,) + chosen_ref.shape[1:], 0)

    def named(owner):
        low = jnp.full(seq_of.shape, NONE, i32)
        for d in range(devices):
            local = every[d] - owner * blocks
            fits = (local >= 0) & (local < blocks) & (owner != d)
            low = jnp.where(fits, jnp.minimum(low, seq_of * blocks + local), low)
        first = jnp.min(low)
        rest = jnp.full(seq_of.shape, NONE, i32)
        for d in range(devices):
            local = every[d] - owner * blocks
            fits = (local >= 0) & (local < blocks) & (owner != d)
            value = seq_of * blocks + local
            rest = jnp.where(fits & (value != first), jnp.minimum(rest, value), rest)
        return first, jnp.min(rest)

    for ask in asks:
        ask.wait_recv()
    mine = named(me)
    for j in range(2):
        for s in range(sequences):
            load(j, s).wait()
    for n in range(CAP):
        block = jnp.where(mine[n] < NONE, mine[n], 0)
        s, place = lax.div(block, blocks), lax.rem(block, blocks)
        pool[me, 0, n] = k[s, place]
        pool[me, 1, n] = v[s, place]

    def own():
        return remote(pool.at[a * 2], pool.at[a * 2], own_send, own_recv, partner)

    def chain(r):
        at = pool.at[(a - r) * 2 + b]
        return remote(at, at, chain_send.at[r], chain_recv.at[r], (a + 1) * 2 + b)

    def arrive(r):
        at = pool.at[(a - r) * 2 + b]
        return remote(at, at, chain_send.at[r - 1], chain_recv.at[r - 1], partner)

    def onto(r, side):
        at = pool.at[(a - r) * 2 + side]
        return remote(at, at, pass_send.at[r - 1], pass_recv.at[r - 1], partner)

    @pl.when(b == 0)
    def _():
        own().start()

    @pl.when(a + 1 < outer)
    def _():
        chain(0).start()

    def relay(r):
        @pl.when(r <= a)
        def _():
            arrive(r).wait_recv()
            onto(r, b).start()

            @pl.when(a + 1 < outer)
            def _():
                chain(r).start()

    dscore[...] = jnp.zeros_like(dscore)

    @pl.loop(0, devices)
    def _(d):
        first, second = named(d)
        table[d * CAP] = jnp.where(d < me, first, NONE)
        table[d * CAP + 1] = jnp.where(d < me, second, NONE)

    spread = lax.broadcasted_iota(i32, (blocks, positions), 1) // BLK == lax.broadcasted_iota(
        i32, (blocks, positions), 0
    )

    def hide_row(asked, block):
        sees = jnp.max(jnp.where(asked == block, 1.0, 0.0), axis=1, keepdims=True)
        sees = jnp.where(spread, sees, 0.0)
        return (1.0 - jnp.sum(sees, axis=0, keepdims=True)) * HIDDEN

    chunk = GROUP * BLK

    @pl.loop(0, sequences)
    def _(s):
        for j in range(2, 5):
            load(j, s).wait()
        for r in range(1, outer):
            @pl.when(s == min(sequences - 1, 1 + (r - 1) * sequences // outer))
            def _(r=r):
                relay(r)
        asked = chosen_ref[s]
        hide = [hide_row(asked, me * blocks + i) for i in range(blocks)]
        for h in range(heads):
            product = g[s, :, head[h]].astype(f32) * o[s, :, head[h]].astype(f32)
            delta_row = jnp.sum(product.T, axis=0, keepdims=True)
            delta[s, h : h + 1] = delta_row
            log_row = log_ref[s, h : h + 1]
            for start in range(0, positions, chunk):
                keys, rest = slice(start // BLK, start // BLK + GROUP), slice(start, positions)
                shift = jnp.concatenate([
                    jnp.broadcast_to((log_row + hide[start // BLK + i])[:, rest], (BLK, positions - start))
                    for i in range(GROUP)
                ], axis=0)
                qq, gg = q[s, rest, head[h]], g[s, rest, head[h]]
                kk = k[s, keys, :, head[h]].reshape(chunk, size)
                vv = v[s, keys, :, head[h]].reshape(chunk, size)
                prob, dsc = probabilities(kk, vv, qq, gg, shift, delta_row[:, rest], scale, True)
                if start == 0:
                    dq[s, :, head[h]] = dot(dsc, kk, TN)
                else:
                    dq[s, rest, head[h]] += dot(dsc, kk, TN)
                tall = (GROUP, BLK, size)
                dk[s, keys, :, head[h]] = (dot(dsc, qq, NN) * scale).astype(bf16).reshape(tall)
                dv[s, keys, :, head[h]] = dot(prob, gg, NN).astype(bf16).reshape(tall)

    def far_terms(owner, at):
        for n in range(CAP):
            ident = table[owner * CAP + n]
            valid = ident < NONE
            ident = jnp.where(valid, ident, 0)
            s = lax.div(ident, blocks)
            block = jnp.where(valid, owner * blocks + lax.rem(ident, blocks), -2)
            hide = hide_row(chosen_ref[s], block)
            logs, deltas = log_ref[s], delta[s]
            for h in range(heads):
                qq, gg = q[s, :, head[h]], g[s, :, head[h]]
                prob, dsc = probabilities(
                    pool[owner, 0, n, :, head[h]], pool[owner, 1, n, :, head[h]], qq, gg,
                    logs[h : h + 1] + hide, deltas[h : h + 1], scale, False,
                )
                dscore[h, pl.ds(pl.multiple_of((at * CAP + n) * BLK, BLK), BLK)] = dsc
                terms[0, owner, n, :, head[h]] = dot(prob, gg, NN).astype(bf16)
                terms[1, owner, n, :, head[h]] = (dot(dsc, qq, NN) * scale).astype(bf16)

    def back(kind, r):
        return remote(
            terms.at[kind, (a - r) * 2 + (1 - b)], back_in.at[kind, r],
            back_send.at[kind, r], back_recv.at[kind, r], partner,
        )

    def home(kind, r):
        return remote(
            back_in.at[kind, r], back_far.at[kind, r - 1],
            home_send.at[kind, r - 1], home_recv.at[kind, r - 1], (a - r) * 2 + b,
        )

    def query_terms(low):
        owners = min(devices - low, BATCH)
        for h in range(heads):
            masked = []
            for s in range(sequences):
                rows = []
                for i in range(owners):
                    for n in range(CAP):
                        ident = table[(low + i) * CAP + n]
                        rows.append(jnp.where(
                            lax.div(ident, blocks) == s, pool[low + i, 0, n, :, head[h]], 0.0
                        ).astype(bf16))
                masked.append(jnp.concatenate(rows, axis=0))
            more = dot(dscore[h], jnp.concatenate(masked, axis=1), TN)
            for s in range(sequences):
                dq[s, :, head[h]] += more[:, s * size : (s + 1) * size]

    @pl.when(b == 1)
    def _():
        own().wait_recv()
        far_terms(a * 2, (a * 2) % BATCH)
        back(0, 0).start()

    @pl.loop(1, a + 1)
    def _(r):
        direct, passed = (a - r) * 2 + b, (a - r) * 2 + (1 - b)
        onto(r, 1 - b).wait_recv()
        far_terms(passed, passed % BATCH)
        back(0, r).start()
        far_terms(direct, direct % BATCH)

    @pl.loop(1 - b, a + 1)
    def _(r):
        back(1, r).start()

    for copy in x_far:
        copy.wait_recv()
    for copy in x_onto:
        copy.start()

    def homeward(kind):
        @pl.loop(1, a + 1)
        def _(r):
            back(kind, r).wait_recv()
            both = terms[kind, (a - r) * 2 + b].astype(f32) + back_in[kind, r].astype(f32)
            back_in[kind, r] = both.astype(bf16)
            home(kind, r).start()

    def settle(kind, rows):
        @pl.when(b == 0)
        def _():
            back(kind, 0).wait_recv()

        @pl.when(b == 1)
        def _():
            back_in[kind, 0] = jnp.zeros(back_in.shape[2:], bf16)

        summed = back_in[kind, 0].astype(f32)
        for r in range(1, outer):
            @pl.when(a + r < outer)
            def _(r=r):
                home(kind, r).wait_recv()

            @pl.when(a + r >= outer)
            def _(r=r):
                back_far[kind, r - 1] = jnp.zeros(back_far.shape[2:], bf16)

            summed += back_far[kind, r - 1].astype(f32)
        fresh = []
        for n in range(CAP):
            block = jnp.where(mine[n] < NONE, mine[n], 0)
            s, place = lax.div(block, blocks), lax.rem(block, blocks)
            fresh.append((rows[s, place].astype(f32) + summed[n]).astype(bf16))
        for s in range(sequences):
            for i in range(blocks):
                value = rows[s, i]
                for n in range(CAP):
                    value = jnp.where(mine[n] == s * blocks + i, fresh[n], value)
                rows[s, i] = value

    homeward(0)
    settle(0, dv)
    put_dv = pltpu.make_async_copy(dv, dv_hbm, out_sem.at[0])
    put_dv.start()

    keep.wait()
    x_own.wait_recv()
    for copy in x_onto:
        copy.wait_recv()
    per = outer // width
    rows_each = dw.shape[0]

    def share(i):
        place = lax.rem(a // per + 1 + i // per, width) * per + i % per
        return place

    def to_partner(i):
        return remote(
            part.at[share(i) * 2 + (1 - b)], part_in.at[i], part_send.at[i], part_recv.at[i], partner
        )

    def to_owner(i, place):
        away = lax.rem(a - place + outer, outer) - 1
        return remote(
            part_in.at[i], part_far.at[away], sum_send.at[i], sum_recv.at[away], place * 2 + b
        )

    for j in range(width):
        from_lane = lax.rem(a // per + 1 + j, width)
        total = dot(x[from_lane].reshape(-1, x.shape[-1]), dv[...].reshape(-1, channels), TN)
        part[pl.ds(from_lane * per * 2, per * 2)] = total.astype(bf16).reshape(per * 2, rows_each, channels)
        for i in range(j * per, (j + 1) * per):
            to_partner(i).start()

    homeward(1)
    for low in range(0, devices, BATCH):
        query_terms(low)
    q[...] = (dq[...] * scale).astype(bf16)
    put_dq = pltpu.make_async_copy(q, dq_hbm, out_sem.at[1])
    put_dq.start()

    for i in range(outer):
        place = share(i)
        to_partner(i).wait_recv()
        both = part[place * 2 + b].astype(f32) + part_in[i].astype(f32)

        @pl.when(place == a)
        def _():
            dw[...] = both

        @pl.when(place != a)
        def _():
            part_in[i] = both.astype(bf16)
            to_owner(i, place).start()

    settle(1, dk)
    put_dk = pltpu.make_async_copy(dk, dk_hbm, out_sem.at[2])
    put_dk.start()

    for r in range(1, outer):
        remote(part_in.at[0], part_far.at[r - 1], sum_send.at[0], sum_recv.at[r - 1], partner).wait_recv()
        dw[...] += part_far[r - 1].astype(f32)
    put_dw = pltpu.make_async_copy(dw, dw_hbm, out_sem.at[3])
    put_dw.start()

    for ask in asks:
        ask.wait_send()
    for copy in x_far + [x_own] + x_onto:
        copy.wait_send()

    @pl.when(b == 0)
    def _():
        own().wait_send()

    for r in range(outer - 1):
        @pl.when((r <= a) & (a + 1 < outer))
        def _(r=r):
            chain(r).wait_send()

    @pl.loop(1, a + 1)
    def _(r):
        onto(r, b).wait_send()
        for kind in range(2):
            home(kind, r).wait_send()

    @pl.loop(1 - b, a + 1)
    def _(r):
        for kind in range(2):
            back(kind, r).wait_send()

    for i in range(outer):
        to_partner(i).wait_send()
        place = share(i)

        @pl.when(place != a)
        def _():
            to_owner(i, place).wait_send()

    for put in (put_dv, put_dq, put_dk, put_dw):
        put.wait()


def body(layer_input, queries, keys, values, outputs, d_out, log_sums, chosen):
    sequences, positions, channels = queries.shape
    features = layer_input.shape[2]
    heads = log_sums.shape[2]
    devices, width = lax.axis_size("kv"), lax.axis_size("tp")
    outer = devices // 2
    rows = width * features // devices
    batch = min(devices, BATCH)
    log_rows = (log_sums * LOG2E).transpose(0, 2, 1)
    dma, vmem = pltpu.SemaphoreType.DMA, pltpu.VMEM
    here, there = pl.BlockSpec(memory_space=pltpu.VMEM), pl.BlockSpec(memory_space=pl.ANY)
    shape = (sequences, positions, channels)
    tall = (sequences, positions // BLK, BLK, channels)
    block = (CAP, BLK, channels)
    d_queries, d_keys, d_values, d_weight = pl.pallas_call(
        functools.partial(kernel, devices, width, heads, (channels // heads) ** (-0.5)),
        in_specs=[there] * 6 + [here] * 2,
        out_specs=[there] * 4,
        out_shape=[
            jax.ShapeDtypeStruct(shape, bf16), jax.ShapeDtypeStruct(tall, bf16),
            jax.ShapeDtypeStruct(tall, bf16), jax.ShapeDtypeStruct((rows, channels), f32),
        ],
        scratch_shapes=[
            vmem((devices,) + chosen.shape, i32),
            vmem(shape, bf16), vmem(tall, bf16), vmem(tall, bf16), vmem(shape, bf16), vmem(shape, bf16),
            vmem((width, sequences, positions, features), bf16),
            vmem(shape, f32), vmem(tall, bf16), vmem(tall, bf16),
            vmem((sequences, heads, positions), f32),
            vmem((devices, 2) + block, bf16),
            vmem((heads, batch * CAP * BLK, positions), bf16),
            vmem((2, devices) + block, bf16),
            vmem((2, outer) + block, bf16),
            vmem((2, outer - 1) + block, bf16),
            vmem((devices, rows, channels), bf16),
            vmem((outer, rows, channels), bf16),
            vmem((outer - 1, rows, channels), bf16),
            vmem((rows, channels), f32),
            pltpu.SMEM((devices * CAP,), i32),
            dma((5, sequences)), dma, dma((4,)), dma((devices - 1,)), dma((devices - 1,)),
            dma((width - 1,)), dma((width - 1,)),
            dma, dma, dma((outer - 1,)), dma((outer - 1,)), dma((outer - 1,)), dma((outer - 1,)),
            dma((2, outer)), dma((2, outer)), dma((2, outer - 1)), dma((2, outer - 1)),
            dma((outer,)), dma((outer,)), dma((outer,)), dma((outer - 1,)),
        ],
        compiler_params=pltpu.CompilerParams(
            collective_id=0, has_side_effects=True, vmem_limit_bytes=67043328
        ),
        name="sparse_backward",
    )(
        layer_input, queries, keys.reshape(tall), values.reshape(tall), outputs, d_out, log_rows, chosen
    )
    return d_queries, d_keys.reshape(shape), d_values.reshape(shape), d_weight


def solution(mesh):
    split = P(None, "kv", "tp")
    return jax.shard_map(
        body,
        mesh=mesh,
        in_specs=(split,) * 7 + (P(None, "kv", None),),
        out_specs=(split, split, split, P("kv", "tp")),
        check_vma=False,
    )
```

time: 183 us -> 109 us (0.60)
  Pallas kernels: 144 us -> 97.8 us
  other arithmetic: 11.8 us -> 1.38 us
  matrix products: 7.35 us -> 0 us
  local copies, waits for them, and re-layouts: 12.4 us -> 7.73 us
  between operations: 4.75 us -> 0.65 us
    pallas_call x5 -> x1, Pallas kernels: 144 us -> 97.8 us  [body(): pl.pallas_call(functools.partial(kernel, devices, width, heads, (channels...]
    dot_general x1 -> x0, matrix products: 7.35 us -> none  [body(): jnp.einsum('pti,tj->pij', input_rows, d_values.reshape(sequences * positi...]
    convert_element_type x1 -> x0, other arithmetic: 4.68 us -> none  [settle(): return rows.astype(bf16).reshape(shape)]
    unnamed x8 -> x10, local copies, waits for them, and re-layouts: 3.21 us -> 7.73 us
    broadcast_in_dim x11 -> x0, local copies, waits for them, and re-layouts: 3.22 us -> none  [the longest x8 2.41 us: settle(): rows = rows + jnp.where(block == served[n], back[n][None], 0.0)]
    reduce_or x4 -> x0, other arithmetic: 2.14 us -> none  [the longest x1 1.4 us: body(): near = jnp.any(chosen[..., None] == mine, axis=2)]
where the time goes in v1:
time: 109 us; the launch traced here: 108 us
  Pallas kernels  97.8 us (90%)
  local copies, waits for them, and re-layouts  7.73 us (7%)
  other arithmetic  1.38 us (1%)
    pallas_call x1, Pallas kernels, body(): pl.pallas_call(functools.partial(kernel, devices, width, heads, (channels...  97.8 us
    unnamed x10, local copies, waits for them, and re-layouts  7.73 us

profile of v1, /device:TPU:10, one launch (start us, length us, event | category | flops | bytes accessed | tf_op | source)
XLA Modules:
  0.0 107.5 jit_solution(3904446511119276002)
XLA Ops:
  0.6 1.4 %multiply_bitcast_fusion.log_ref = f32[4,4,512]{2,1,0:T(4,128)} fusion(f32[4,512,4]{1,2,0:T(4,128)} %param.14), kind=kLoop, calls=%fused_computation | loop fusion | flops 8192 | bytes 65536 | tf_op jit(solution)/shard_map/transpose | solution.py:438
  2.0 97.8 %sparse_backward.1 = (bf16[4,512,512]{2,1,0:T(8,128)(2,1)}, bf16[4,8,64,512]{3,2,1,0:T(8,128)(2,1)}, bf16[4,8,64,512]{3,2,1,0:T(8,128)(2,1)}, f32[256,512]{1,0:T(8,128)}) custom-call(bf16[4,512,512]{2,1,0:T(8,128)(2,1)} %x_hbm.1, bf16[4,512,512]{2,1,0:T(8,128)(2,1)} %q_hbm.1, bf16[4,8,64,512]{3,2,1,0:T(8,128)(2,1)} %bitcast.8, ...), custom_call_target="tpu_custom_call" | custom-call | tf_op jit(solution)/shard_map/sparse_backward/pallas_call | solution.py:444
  99.8 0.0 copy-start.1
  99.8 3.2 %copy.16 = bf16[4,512,512]{2,1,0:T(8,128)(2,1)} copy(bf16[4,512,512]{2,1,0:T(8,128)(2,1)} %get-tuple-element.16) | data formatting | bytes 4194304
  103.0 0.0 copy-done.1
  103.0 0.0 copy-start
  103.0 1.3 %copy.17 = bf16[4,512,512]{2,1,0:T(8,128)(2,1)} copy(bf16[4,512,512]{2,1,0:T(8,128)(2,1)S(1)} %bitcast.7) | data formatting | bytes 4194304
  104.3 1.0 copy-done
  105.3 0.0 copy-start.2
  105.3 1.3 %copy.18 = bf16[4,512,512]{2,1,0:T(8,128)(2,1)} copy(bf16[4,512,512]{2,1,0:T(8,128)(2,1)S(1)} %bitcast.6) | data formatting | bytes 4194304
  106.7 0.1 copy-done.2
  106.7 0.8 copy.19
Async XLA Ops:
  99.8 3.2 %copy-start.1 = (bf16[4,8,64,512]{3,2,1,0:T(8,128)(2,1)S(1)}, bf16[4,8,64,512]{3,2,1,0:T(8,128)(2,1)}, u32[]{:S(2)}) copy-start(bf16[4,8,64,512]{3,2,1,0:T(8,128)(2,1)} %get-tuple-element.9) | copy-start | bytes 6291460
  103.0 2.3 %copy-start = (bf16[4,8,64,512]{3,2,1,0:T(8,128)(2,1)S(1)}, bf16[4,8,64,512]{3,2,1,0:T(8,128)(2,1)}, u32[]{:S(2)}) copy-start(bf16[4,8,64,512]{3,2,1,0:T(8,128)(2,1)} %get-tuple-element.10) | copy-start | bytes 6291460
  105.3 1.4 %copy-start.2 = (f32[256,512]{1,0:T(8,128)S(1)}, f32[256,512]{1,0:T(8,128)}, u32[]{:S(2)}) copy-start(f32[256,512]{1,0:T(8,128)} %get-tuple-element.19) | copy-start | bytes 1572868

commit v2 on v1

--- a/solution.py
+++ b/solution.py
@@ -13,6 +13,7 @@
 HIDDEN = 1e30
 GROUP = 4
 BATCH = 8
+PIECES = 2
 NONE = 1 << 20
 
 NT = (((1,), (1,)), ((), ()))
@@ -48,10 +49,10 @@
     x_hbm, q_hbm, k_hbm, v_hbm, o_hbm, g_hbm, log_ref, chosen_ref,
     dq_hbm, dk_hbm, dv_hbm, dw_hbm,
     every, q, k, v, o, g, x, dq, dk, dv, delta, pool, dscore, terms, back_in, back_far, part, part_in,
-    part_far, dw, table,
+    part_far, pair_in, dw, table,
     load_sem, keep_sem, out_sem, every_send, every_recv, x_send, x_recv,
     own_send, own_recv, chain_send, chain_recv, pass_send, pass_recv,
-    back_send, back_recv, home_send, home_recv, part_send, part_recv, sum_send, sum_recv,
+    back_send, back_recv, home_send, home_recv, part_send, part_recv, sum_send, sum_recv, pair_recv,
 ):
     sequences, positions, channels = q.shape
     size = channels // heads
@@ -195,7 +196,7 @@
             product = g[s, :, head[h]].astype(f32) * o[s, :, head[h]].astype(f32)
             delta_row = jnp.sum(product.T, axis=0, keepdims=True)
             delta[s, h : h + 1] = delta_row
-            log_row = log_ref[s, h : h + 1]
+            log_row = log_ref[s, h : h + 1] * LOG2E
             for start in range(0, positions, chunk):
                 keys, rest = slice(start // BLK, start // BLK + GROUP), slice(start, positions)
                 shift = jnp.concatenate([
@@ -222,7 +223,7 @@
             s = lax.div(ident, blocks)
             block = jnp.where(valid, owner * blocks + lax.rem(ident, blocks), -2)
             hide = hide_row(chosen_ref[s], block)
-            logs, deltas = log_ref[s], delta[s]
+            logs, deltas = log_ref[s] * LOG2E, delta[s]
             for h in range(heads):
                 qq, gg = q[s, :, head[h]], g[s, :, head[h]]
                 prob, dsc = probabilities(
@@ -280,11 +281,6 @@
     def _(r):
         back(1, r).start()
 
-    for copy in x_far:
-        copy.wait_recv()
-    for copy in x_onto:
-        copy.start()
-
     def homeward(kind):
         @pl.loop(1, a + 1)
         def _(r):
@@ -330,63 +326,95 @@
     put_dv = pltpu.make_async_copy(dv, dv_hbm, out_sem.at[0])
     put_dv.start()
 
-    keep.wait()
-    x_own.wait_recv()
-    for copy in x_onto:
-        copy.wait_recv()
     per = outer // width
-    rows_each = dw.shape[0]
-
-    def share(i):
-        place = lax.rem(a // per + 1 + i // per, width) * per + i % per
-        return place
-
-    def to_partner(i):
-        return remote(
-            part.at[share(i) * 2 + (1 - b)], part_in.at[i], part_send.at[i], part_recv.at[i], partner
-        )
-
-    def to_owner(i, place):
-        away = lax.rem(a - place + outer, outer) - 1
-        return remote(
-            part_in.at[i], part_far.at[away], sum_send.at[i], sum_recv.at[away], place * 2 + b
-        )
+    rows_each = dw.shape[1]
+
+    def from_lane(j):
+        return lax.rem((lane if j % 2 == 0 else core) + width - j // 2 * 2, width)
+
+    def share(t):
+        i = t // PIECES
+        return from_lane(i // per) * per + i % per
+
+    def to_partner(t):
+        source = (share(t) * 2 + (1 - b)) * PIECES + t % PIECES
+        return remote(part.at[source], part_in.at[t], part_send.at[t], part_recv.at[t], partner)
+
+    def to_owner(t, place):
+        at = (lax.rem(a - place + outer, outer) - 1) * PIECES + t % PIECES
+        return remote(part_in.at[t], part_far.at[at], sum_send.at[t], sum_recv.at[at], place * 2 + b)
+
+    half = outer // 2
+    paired = outer == 4
+    inner = (a == half - 1) | (a == half)
+
+    def to_inner(t, chip):
+        return remote(part_in.at[t], pair_in.at[t], sum_send.at[t], pair_recv.at[t], chip)
 
     for j in range(width):
-        from_lane = lax.rem(a // per + 1 + j, width)
-        total = dot(x[from_lane].reshape(-1, x.shape[-1]), dv[...].reshape(-1, channels), TN)
-        part[pl.ds(from_lane * per * 2, per * 2)] = total.astype(bf16).reshape(per * 2, rows_each, channels)
-        for i in range(j * per, (j + 1) * per):
-            to_partner(i).start()
+        if j == 0:
+            keep.wait()
+        elif j == 1:
+            x_own.wait_recv()
+        elif j % 2 == 0:
+            x_far[j // 2 - 1].wait_recv()
+            x_onto[j // 2 - 1].start()
+        else:
+            x_onto[j // 2 - 1].wait_recv()
+        total = dot(x[from_lane(j)].reshape(-1, x.shape[-1]), dv[...].reshape(-1, channels), TN)
+        many = per * 2 * PIECES
+        part[pl.ds(from_lane(j) * many, many)] = total.astype(bf16).reshape(many, rows_each, channels)
+        for t in range(j * per * PIECES, (j + 1) * per * PIECES):
+            to_partner(t).start()
 
     homeward(1)
+    for t in range(outer * PIECES):
+        place = share(t)
+        to_partner(t).wait_recv()
+        both = part[(place * 2 + b) * PIECES + t % PIECES].astype(f32) + part_in[t].astype(f32)
+        crossing = ((place < half) != (a < half)) & paired
+
+        @pl.when(place == a)
+        def _():
+            dw[t % PIECES] = both
+
+        @pl.when((place != a) & jnp.logical_not(crossing))
+        def _():
+            part_in[t] = both.astype(bf16)
+            to_owner(t, place).start()
+
+        if paired:
+            @pl.when(crossing & inner)
+            def _():
+                to_inner(t, partner).wait_recv()
+                part_in[t] = (both + pair_in[t].astype(f32)).astype(bf16)
+                to_owner(t, place).start()
+
+            @pl.when(crossing & jnp.logical_not(inner))
+            def _():
+                part_in[t] = both.astype(bf16)
+                to_inner(t, jnp.where(a < half, half - 1, half) * 2 + b).start()
+
     for low in range(0, devices, BATCH):
         query_terms(low)
     q[...] = (dq[...] * scale).astype(bf16)
     put_dq = pltpu.make_async_copy(q, dq_hbm, out_sem.at[1])
     put_dq.start()
 
-    for i in range(outer):
-        place = share(i)
-        to_partner(i).wait_recv()
-        both = part[place * 2 + b].astype(f32) + part_in[i].astype(f32)
-
-        @pl.when(place == a)
-        def _():
-            dw[...] = both
-
-        @pl.when(place != a)
-        def _():
-            part_in[i] = both.astype(bf16)
-            to_owner(i, place).start()
-
     settle(1, dk)
     put_dk = pltpu.make_async_copy(dk, dk_hbm, out_sem.at[2])
     put_dk.start()
 
-    for r in range(1, outer):
-        remote(part_in.at[0], part_far.at[r - 1], sum_send.at[0], sum_recv.at[r - 1], partner).wait_recv()
-        dw[...] += part_far[r - 1].astype(f32)
+    for c in range(PIECES):
+        for r in range(1, outer):
+            source = lax.rem(a + r, outer)
+            near = (source < half) == (a < half)
+            at = (r - 1) * PIECES + c
+
+            @pl.when(near | (source == half - 1) | (source == half) | (not paired))
+            def _(at=at, c=c):
+                remote(part_in.at[0], part_far.at[at], sum_send.at[0], sum_recv.at[at], partner).wait_recv()
+                dw[c] += part_far[at].astype(f32)
     put_dw = pltpu.make_async_copy(dw, dw_hbm, out_sem.at[3])
     put_dw.start()
 
@@ -415,13 +443,13 @@
         for kind in range(2):
             back(kind, r).wait_send()
 
-    for i in range(outer):
-        to_partner(i).wait_send()
-        place = share(i)
+    for t in range(outer * PIECES):
+        to_partner(t).wait_send()
+        place = share(t)
 
         @pl.when(place != a)
         def _():
-            to_owner(i, place).wait_send()
+            to_inner(t, partner).wait_send()
 
     for put in (put_dv, put_dq, put_dk, put_dw):
         put.wait()
@@ -435,19 +463,20 @@
     outer = devices // 2
     rows = width * features // devices
     batch = min(devices, BATCH)
-    log_rows = (log_sums * LOG2E).transpose(0, 2, 1)
+    log_rows = log_sums.transpose(0, 2, 1)
     dma, vmem = pltpu.SemaphoreType.DMA, pltpu.VMEM
     here, there = pl.BlockSpec(memory_space=pltpu.VMEM), pl.BlockSpec(memory_space=pl.ANY)
     shape = (sequences, positions, channels)
     tall = (sequences, positions // BLK, BLK, channels)
     block = (CAP, BLK, channels)
+    piece = (rows // PIECES, channels)
     d_queries, d_keys, d_values, d_weight = pl.pallas_call(
         functools.partial(kernel, devices, width, heads, (channels // heads) ** (-0.5)),
         in_specs=[there] * 6 + [here] * 2,
         out_specs=[there] * 4,
         out_shape=[
             jax.ShapeDtypeStruct(shape, bf16), jax.ShapeDtypeStruct(tall, bf16),
-            jax.ShapeDtypeStruct(tall, bf16), jax.ShapeDtypeStruct((rows, channels), f32),
+            jax.ShapeDtypeStruct(tall, bf16), jax.ShapeDtypeStruct((PIECES,) + piece, f32),
         ],
         scratch_shapes=[
             vmem((devices,) + chosen.shape, i32),
@@ -460,25 +489,26 @@
             vmem((2, devices) + block, bf16),
             vmem((2, outer) + block, bf16),
             vmem((2, outer - 1) + block, bf16),
-            vmem((devices, rows, channels), bf16),
-            vmem((outer, rows, channels), bf16),
-            vmem((outer - 1, rows, channels), bf16),
-            vmem((rows, channels), f32),
+            vmem((devices * PIECES,) + piece, bf16),
+            vmem((outer * PIECES,) + piece, bf16),
+            vmem(((outer - 1) * PIECES,) + piece, bf16),
+            vmem((outer * PIECES if outer == 4 else 1,) + piece, bf16),
+            vmem((PIECES,) + piece, f32),
             pltpu.SMEM((devices * CAP,), i32),
             dma((5, sequences)), dma, dma((4,)), dma((devices - 1,)), dma((devices - 1,)),
             dma((width - 1,)), dma((width - 1,)),
             dma, dma, dma((outer - 1,)), dma((outer - 1,)), dma((outer - 1,)), dma((outer - 1,)),
             dma((2, outer)), dma((2, outer)), dma((2, outer - 1)), dma((2, outer - 1)),
-            dma((outer,)), dma((outer,)), dma((outer,)), dma((outer - 1,)),
+            *[dma((outer * PIECES,))] * 3, dma(((outer - 1) * PIECES,)), dma((outer * PIECES,)),
         ],
         compiler_params=pltpu.CompilerParams(
-            collective_id=0, has_side_effects=True, vmem_limit_bytes=67043328
+            collective_id=0, has_side_effects=True, vmem_limit_bytes=min(67043328, (34 * 2 + 3 * devices) * 2**19)
         ),
         name="sparse_backward",
     )(
         layer_input, queries, keys.reshape(tall), values.reshape(tall), outputs, d_out, log_rows, chosen
     )
-    return d_queries, d_keys.reshape(shape), d_values.reshape(shape), d_weight
+    return d_queries, d_keys.reshape(shape), d_values.reshape(shape), d_weight.reshape(rows, channels)
 
 
 def solution(mesh):

time: 109 us -> 98.3 us (0.902); the launches traced: 108 us -> 98 us
  Pallas kernels: 97.8 us -> 91.2 us
  local copies, waits for them, and re-layouts: 7.73 us -> 6.22 us
  other arithmetic: 1.38 us -> 0 us
    pallas_call x1, Pallas kernels: 97.8 us -> 91.2 us  [body(): pl.pallas_call(functools.partial(kernel, devices, width, heads, (channels...]
    unnamed x10 -> x8, local copies, waits for them, and re-layouts: 7.73 us -> 6.22 us
    transpose x1 -> x0, other arithmetic: 1.38 us -> none  [body(): log_rows = (log_sums * LOG2E).transpose(0, 2, 1)]
where the time goes in v2:
time: 98.3 us; the launch traced here: 98 us
  Pallas kernels  91.2 us (93%)
  local copies, waits for them, and re-layouts  6.22 us (6%)
    pallas_call x1, Pallas kernels, body(): pl.pallas_call(functools.partial(kernel, devices, width, heads, (channels...  91.2 us
    unnamed x8, local copies, waits for them, and re-layouts  6.22 us

profile of v2, /device:TPU:10, one launch (start us, length us, event | category | flops | bytes accessed | tf_op | source)
XLA Modules:
  0.0 98.0 jit_solution(16395280481975764818)
XLA Ops:
  0.6 0.0 copy-start
  0.6 0.7 copy-done
  1.4 0.0 copy-start.1
  1.4 0.7 copy-done.1
  2.1 91.2 %sparse_backward.1 = (bf16[4,512,512]{2,1,0:T(8,128)(2,1)S(1)}, bf16[4,8,64,512]{3,2,1,0:T(8,128)(2,1)S(1)}, bf16[4,8,64,512]{3,2,1,0:T(8,128)(2,1)S(1)}, f32[2,128,512]{2,1,0:T(8,128)S(1)}) custom-call(bf16[4,512,512]{2,1,0:T(8,128)(2,1)} %x_hbm.1, bf16[4,512,512]{2,1,0:T(8,128)(2,1)} %q_hbm.1, bf16[4,8,64,512]{3,2,1,0:T(8,128)(2,1)} %bitcast.10, ...), custom_call_target="tpu_custom_call" | custom-call | tf_op jit(solution)/shard_map/sparse_backward/pallas_call | solution.py:473
  93.3 1.3 %copy.16 = bf16[4,512,512]{2,1,0:T(8,128)(2,1)} copy(bf16[4,512,512]{2,1,0:T(8,128)(2,1)S(1)} %get-tuple-element.16) | data formatting | bytes 4194304
  94.6 1.3 %copy.17 = bf16[4,512,512]{2,1,0:T(8,128)(2,1)} copy(bf16[4,512,512]{2,1,0:T(8,128)(2,1)S(1)} %bitcast.7) | data formatting | bytes 4194304
  95.9 1.3 %copy.18 = bf16[4,512,512]{2,1,0:T(8,128)(2,1)} copy(bf16[4,512,512]{2,1,0:T(8,128)(2,1)S(1)} %bitcast.6) | data formatting | bytes 4194304
  97.3 0.8 copy.19
Async XLA Ops:
  0.6 0.8 copy-start
  1.4 0.7 copy-start.1
